TPU v7x, 512 devices: a whole 4x4x16 slice. The times are simulated.
512 devices in a mesh: sp: 32 (over z, core), tp: 16 (over y, x).
Axes of the slice: x: 4, y: 4, z: 16, core: 2. Of those that a mesh axis runs over, the one named last changes fastest.
Arguments:
- layer_input: bfloat16 [32768, 4096], P('sp', 'tp'), may hold values from -6 to 6
- key_weight: bfloat16 [4096, 4096], P(None, 'tp'), may hold values from -0.09375 to 0.09375
- value_weight: bfloat16 [4096, 4096], P(None, 'tp'), may hold values from -0.09375 to 0.09375
- decay_exponent: float32 [32], P('tp'), may hold values from -0.077 to -4.2114258e-05, as said below
- query_new: bfloat16 [2, 4096], P(None, 'tp'), may hold values from -6 to 6
- key_new: bfloat16 [2, 4096], P(None, 'tp'), may hold values from -6 to 6
- value_new: bfloat16 [2, 4096], P(None, 'tp'), may hold values from -6 to 6
- norm_gain: float32 [4096], P('tp'), may hold values from 0.1 to 1.9
Outputs:
- state_cache: bfloat16 [2, 32, 128, 128], P(None, 'tp', 'sp')
- first_read: bfloat16 [2, 4096], P(None, 'tp')
Inputs may be any that keep to these rules, and one draw needn't show every extreme that they name: decay_exponent is negative.
All inputs are finite; a program needn't handle non-finite values.
Results may differ from a plain program's by a relative error of at most 0.011.
Values may be sent and summed in bfloat16 or wider, within the bound.
A program may use at most 64 MiB of HBM per device.

v0:
```python
import jax
import jax.numpy as jnp
from jax import lax
from jax.sharding import PartitionSpec as P

SEQS = 2


def in_blocks(x, dim, peers):
    before, after = (x.shape[:dim], x.shape[dim + 1 :])
    return jnp.moveaxis(x.reshape(*before, peers, -1, *after), dim, 0)


def sent_and_summed(x, axis, dim):
    tiles = in_blocks(x, dim, lax.axis_size(axis))
    arrived = lax.all_to_all(tiles, axis, split_axis=0, concat_axis=0, tiled=True)
    return arrived.astype(jnp.float32).sum(axis=0)


def copy_for_each(x, axis):
    copies = jnp.broadcast_to(x, (lax.axis_size(axis), *x.shape))
    return lax.all_to_all(copies, axis, split_axis=0, concat_axis=0, tiled=True)


def of_everyone(x, axis):
    return copy_for_each(x, axis).sum(axis=0)


def rotate(projected, position):
    half_width = projected.shape[-1] // 2
    inverse = 1.0 / 10000.0 ** jnp.linspace(0.0, 1.0, half_width, dtype=jnp.float32)
    angle = position[:, None] * inverse[None, :]
    cosine = jnp.cos(angle)[:, None, :]
    sine = jnp.sin(angle)[:, None, :]
    first = projected[..., :half_width]
    second = projected[..., half_width:]
    return jnp.concatenate(
        [first * cosine - second * sine, first * sine + second * cosine], axis=-1
    )


def on_device(
    layer_input, key_weight, value_weight, decay_exponent, query_new, key_new, value_new, norm_gain
):
    tok_count = layer_input.shape[0]
    head_local = decay_exponent.shape[0]
    key_width = key_weight.shape[1] // head_local
    value_width = value_weight.shape[1] // head_local
    seq_span = lax.axis_size("sp") // SEQS
    seq_length = tok_count * seq_span
    sp_place = lax.axis_index("sp")
    feature_block = lax.all_gather(layer_input, "tp", axis=1, tiled=True)
    key_proj = jnp.dot(feature_block, key_weight, preferred_element_type=jnp.float32)
    value_proj = jnp.dot(feature_block, value_weight, preferred_element_type=jnp.float32)
    position = (sp_place % seq_span * tok_count + jnp.arange(tok_count, dtype=jnp.int32)).astype(
        jnp.float32
    )
    keys = (
        rotate(key_proj.reshape(tok_count, head_local, key_width), position) * key_width ** (-0.5)
    ).astype(jnp.bfloat16)
    values = value_proj.astype(jnp.bfloat16).reshape(tok_count, head_local, value_width)
    distance = seq_length - 1.0 - position
    weighting = jnp.exp(decay_exponent[None, :] * distance[:, None])
    weighted = (keys.astype(jnp.float32) * weighting[:, :, None]).astype(jnp.bfloat16)
    local_state = jnp.einsum("thd,the->hde", weighted, values, preferred_element_type=jnp.float32)
    member = (jnp.arange(SEQS, dtype=jnp.int32) == sp_place // seq_span).astype(jnp.float32)
    state_terms = member[:, None, None, None] * local_state[None]
    final_rows = sent_and_summed(state_terms.astype(jnp.bfloat16), "sp", 2)
    state_cache = final_rows.astype(jnp.bfloat16)
    queries = query_new.astype(jnp.float32).reshape(SEQS, head_local, key_width)
    partial_read = jnp.einsum(
        "shd,shde->she", queries, state_terms, precision=lax.Precision.HIGHEST
    )
    carried = of_everyone(partial_read, "sp")
    keys_next = key_new.astype(jnp.float32).reshape(SEQS, head_local, key_width)
    values_next = value_new.astype(jnp.float32).reshape(SEQS, head_local, value_width)
    own_term = jnp.sum(queries * keys_next, axis=2)[:, :, None] * values_next
    mixed = jnp.exp(decay_exponent)[None, :, None] * carried + own_term
    normed = mixed * lax.rsqrt(jnp.mean(mixed * mixed, axis=2, keepdims=True) + 1e-06)
    normed = normed * norm_gain.reshape(head_local, value_width)[None, :, :]
    return (state_cache, normed.reshape(SEQS, head_local * value_width).astype(jnp.bfloat16))


def solution(mesh):
    in_specs = (
        P("sp", "tp"),
        P(None, "tp"),
        P(None, "tp"),
        P("tp"),
        P(None, "tp"),
        P(None, "tp"),
        P(None, "tp"),
        P("tp"),
    )
    out_specs = (P(None, "tp", "sp", None), P(None, "tp"))
    return jax.shard_map(
        on_device, mesh=mesh, in_specs=in_specs, out_specs=out_specs, check_vma=False
    )
```

profile of v0, /device:TPU:1, one launch (start us, length us, event | category | flops | bytes accessed | tf_op | source)
XLA Modules:
  0.0 174.9 jit_solution(16979299565072083331)
XLA Ops:
  7.2 0.0 copy-start
  7.2 0.0 all-gather.2.cloned.1.call-start
  7.2 0.7 all-gather.2.cloned.1.call-update
  7.9 0.7 reshape.155
  8.6 0.7 exp.11
  9.3 0.1 fusion.12
  9.4 0.7 convert_multiply_fusion
  10.1 0.7 multiply_exponential_fusion
  10.8 1.0 multiply_cosine_fusion
  11.8 95.6 %all-gather.2.cloned.1.call-done = bf16[1024,4096]{1,0:T(8,128)(2,1)} async-done(((bf16[1024,256]{1,0:T(8,128)(2,1)}), bf16[1024,4096]{1,0:T(8,128)(2,1)}) %all-gather.2.cloned.1.call-update) | async-done | bytes 8388624 | tf_op jit(solution)/shard_map/all_gather | solution.py:52
  107.5 0.0 copy-done
  107.5 0.0 copy-start.3
  107.5 5.9 %fusion.15 = f32[1024,256]{0,1:T(8,128)S(1)} fusion(bf16[1024,4096]{1,0:T(8,128)(2,1)} %all-gather.2.cloned.1.call-done, bf16[4096,256]{1,0:T(8,128)(2,1)S(1)} %copy-done), kind=kOutput, calls=%fused_computation.37 | convolution fusion | flops 2147483648 | bytes 11534336 | tf_op jit(solution)/shard_map/dot_general | solution.py:53
  113.4 0.0 copy-start.4
  113.4 0.2 multiply_subtract_fusion
  113.5 0.0 copy-done.3
  113.6 1.4 copy-done.4
  115.0 2.4 %convolution_convert_fusion = bf16[1024,256]{0,1:T(8,128)(2,1)S(1)} fusion(bf16[1024,4096]{1,0:T(8,128)(2,1)S(1)} %copy-done.3, bf16[4096,256]{1,0:T(8,128)(2,1)S(1)} %copy-done.4), kind=kOutput, calls=%fused_computation | convolution fusion | flops 2147745792 | bytes 11010048 | tf_op jit(solution)/shard_map/dot_general | solution.py:54
  117.4 0.0 copy-start.1
  117.4 0.0 copy-start.2
  117.4 0.3 fusion.1
  117.7 0.3 fusion.5
  118.0 0.6 broadcast_in_dim.4
  118.7 14.4 %all-to-all-start.1 = ((f32[32,2,2,128]{3,2,1,0:T(2,128)}), f32[32,2,2,128]{3,2,1,0:T(2,128)S(1)}, u32[]{:S(2)}, u32[]{:S(2)}) async-start(f32[32,2,2,128]{3,2,1,0:T(2,128)} %broadcast_in_dim.4), calls=%async_computation.1 | async-start | bytes 131072 | tf_op jit(solution)/shard_map/all_to_all | solution.py:22
  133.1 0.1 broadcast_bitcast_fusion.2
  133.1 0.0 copy-done.1
  133.2 0.1 reduce_sum.44
  133.2 0.8 multiply_convert_fusion.2
  134.0 12.1 %all-to-all-done.1 = f32[32,2,2,128]{3,2,1,0:T(2,128)S(1)} async-done(((f32[32,2,2,128]{3,2,1,0:T(2,128)}), f32[32,2,2,128]{3,2,1,0:T(2,128)S(1)}, u32[]{:S(2)}, u32[]{:S(2)}) %all-to-all-start.1) | async-done | bytes 65568 | tf_op jit(solution)/shard_map/all_to_all | solution.py:22
  146.1 5.1 %all-to-all-start = ((bf16[32,2,2,4,128]{4,3,2,1,0:T(4,128)(2,1)}), bf16[32,2,2,4,128]{4,3,2,1,0:T(4,128)(2,1)S(1)}, u32[]{:S(2)}, u32[]{:S(2)}) async-start(bf16[32,2,2,4,128]{4,3,2,1,0:T(4,128)(2,1)} %multiply_convert_fusion.2), calls=%async_computation | async-start | bytes 262144 | tf_op jit(solution)/shard_map/all_to_all | solution.py:16
  151.2 0.2 broadcast_bitcast_fusion.1
  151.4 0.1 broadcast_bitcast_fusion
  151.5 0.0 copy-done.2
  151.5 0.6 fusion.10
  152.0 15.3 %all-to-all-done = bf16[32,2,2,4,128]{4,3,2,1,0:T(4,128)(2,1)S(1)} async-done(((bf16[32,2,2,4,128]{4,3,2,1,0:T(4,128)(2,1)}), bf16[32,2,2,4,128]{4,3,2,1,0:T(4,128)(2,1)S(1)}, u32[]{:S(2)}, u32[]{:S(2)}) %all-to-all-start) | async-done | bytes 131104 | tf_op jit(solution)/shard_map/all_to_all | solution.py:16
  167.4 0.7 reduce_sum.41
  (8 shorter events, 0.1 us)
Async XLA Ops:
  7.2 100.3 %copy-start = (bf16[4096,256]{1,0:T(8,128)(2,1)S(1)}, bf16[4096,256]{1,0:T(8,128)(2,1)}, u32[]{:S(2)}) copy-start(bf16[4096,256]{1,0:T(8,128)(2,1)} %param.9) | copy-start | bytes 6291460
  7.2 100.3 %all-gather.2.cloned.1.call-start = ((), (), s32[]{:S(2)}) async-start(), calls=%async_computation.2 | async-start | bytes 8912896 | tf_op jit(solution)/shard_map/all_gather | solution.py:52
  107.5 6.1 %copy-start.3 = (bf16[1024,4096]{1,0:T(8,128)(2,1)S(1)}, bf16[1024,4096]{1,0:T(8,128)(2,1)}, u32[]{:S(2)}) copy-start(bf16[1024,4096]{1,0:T(8,128)(2,1)} %all-gather.2.cloned.1.call-done) | copy-start | bytes 25165828
  113.4 1.6 copy-start.4
  117.4 15.8 %copy-start.1 = (bf16[2,256]{1,0:T(2,128)(2,1)S(1)}, bf16[2,256]{1,0:T(2,128)(2,1)}, u32[]{:S(2)}) copy-start(bf16[2,256]{1,0:T(2,128)(2,1)} %param.14) | copy-start | bytes 3076
  117.4 34.1 %copy-start.2 = (f32[256]{0:T(256)S(1)}, f32[256]{0:T(256)}, u32[]{:S(2)}) copy-start(f32[256]{0:T(256)} %param.15) | copy-start | bytes 3076
  118.7 27.4 %all-to-all-start.1 = ((f32[32,2,2,128]{3,2,1,0:T(2,128)}), f32[32,2,2,128]{3,2,1,0:T(2,128)S(1)}, u32[]{:S(2)}, u32[]{:S(2)}) async-start(f32[32,2,2,128]{3,2,1,0:T(2,128)} %broadcast_in_dim.4), calls=%async_computation.1 | async-start | bytes 131072 | tf_op jit(solution)/shard_map/all_to_all | solution.py:22
  146.1 21.3 %all-to-all-start = ((bf16[32,2,2,4,128]{4,3,2,1,0:T(4,128)(2,1)}), bf16[32,2,2,4,128]{4,3,2,1,0:T(4,128)(2,1)S(1)}, u32[]{:S(2)}, u32[]{:S(2)}) async-start(bf16[32,2,2,4,128]{4,3,2,1,0:T(4,128)(2,1)} %multiply_convert_fusion.2), calls=%async_computation | async-start | bytes 262144 | tf_op jit(solution)/shard_map/all_to_all | solution.py:16
Sparse Core Ops, SparseCore 0:
  11.0 96.4 all-gather.1
where the time goes:
time: 175 us
  waiting for transfers between devices  124 us (71%)
  starting transfers between devices  19.5 us (11%)
  between operations  14.2 us (8%)
  matrix products  8.92 us (5%)
  other arithmetic  4.99 us (3%)
  local copies, waits for them, and re-layouts  3.61 us (2%)
    all_gather x1, waiting for transfers between devices, on_device(): feature_block = lax.all_gather(layer_input, 'tp', axis=1, tiled=True)  95.6 us
    all_to_all x1, waiting for transfers between devices, sent_and_summed(): lax.all_to_all(tiles, axis, split_axis=0, concat_axis=0, tiled=True)  15.3 us
    all_to_all x1, starting transfers between devices, copy_for_each(): return lax.all_to_all(copies, axis, split_axis=0, concat_axis=0, tiled=True)  14.4 us
    all_to_all x1, waiting for transfers between devices, copy_for_each(): return lax.all_to_all(copies, axis, split_axis=0, concat_axis=0, tiled=True)  12.1 us
    dot_general x1, matrix products, on_device(): jnp.dot(feature_block, key_weight, preferred_element_type=jnp.float32)  5.9 us
    all_to_all x1, starting transfers between devices, sent_and_summed(): lax.all_to_all(tiles, axis, split_axis=0, concat_axis=0, tiled=True)  5.1 us
  transfers between devices with their start and end apart: 3, of which 3 were waited for; matrix products, arithmetic and copies ran while one was open for 3% of the time, Pallas kernels for 0%

commit v1 on v0

--- a/solution.py
+++ b/solution.py
@@ -49,7 +49,7 @@
     seq_span = lax.axis_size("sp") // SEQS
     seq_length = tok_count * seq_span
     sp_place = lax.axis_index("sp")
-    feature_block = lax.all_gather(layer_input, "tp", axis=1, tiled=True)
+    feature_block = jnp.concatenate(lax.all_gather(layer_input, "tp"), axis=1)
     key_proj = jnp.dot(feature_block, key_weight, preferred_element_type=jnp.float32)
     value_proj = jnp.dot(feature_block, value_weight, preferred_element_type=jnp.float32)
     position = (sp_place % seq_span * tok_count + jnp.arange(tok_count, dtype=jnp.int32)).astype(

time: 175 us -> 201 us (1.15)
  local copies, waits for them, and re-layouts: 3.61 us -> 39.4 us
  waiting for transfers between devices: 124 us -> 114 us
    reshape x0 -> x1, local copies, waits for them, and re-layouts: none -> 13.5 us  [on_device(): feature_block = jnp.concatenate(lax.all_gather(layer_input, 'tp'), axis=1)]
    all_gather x0 -> x1, local copies, waits for them, and re-layouts: none -> 11.4 us  [on_device(): feature_block = jnp.concatenate(lax.all_gather(layer_input, 'tp'), axis=1)]
    all_gather x1, waiting for transfers between devices: 95.6 us -> 86.3 us  [on_device(): feature_block = jnp.concatenate(lax.all_gather(layer_input, 'tp'), axis=1)]
    unnamed x11 -> x12, local copies, waits for them, and re-layouts: 1.51 us -> 8.3 us
    dot_general x0 -> x1, local copies, waits for them, and re-layouts: none -> 4.13 us  [on_device(): jnp.dot(feature_block, key_weight, preferred_element_type=jnp.float32)]
    dot_general x1, matrix products: 5.9 us -> 2.36 us  [on_device(): jnp.dot(feature_block, key_weight, preferred_element_type=jnp.float32)]
    dot_general x1, matrix products: 2.41 us -> 5.9 us  [on_device(): jnp.dot(feature_block, value_weight, preferred_element_type=jnp.float32)]
  transfers between devices with their start and end apart: 3 -> 3, of which waited for: 3 -> 3; matrix products, arithmetic and copies ran while one was open for 3% -> 5% of each run, Pallas kernels for 0% -> 0%
where the time goes in v1:
time: 201 us; the launch traced here: 200 us
  waiting for transfers between devices  114 us (57%)
  local copies, waits for them, and re-layouts  39.4 us (20%)
  starting transfers between devices  18.3 us (9%)
  between operations  14.1 us (7%)
  matrix products  8.88 us (4%)
  other arithmetic  4.99 us (2%)
    all_gather x1, waiting for transfers between devices, on_device(): feature_block = jnp.concatenate(lax.all_gather(layer_input, 'tp'), axis=1)  86.3 us
    all_to_all x1, waiting for transfers between devices, sent_and_summed(): lax.all_to_all(tiles, axis, split_axis=0, concat_axis=0, tiled=True)  15.3 us
    reshape x1, local copies, waits for them, and re-layouts, on_device(): feature_block = jnp.concatenate(lax.all_gather(layer_input, 'tp'), axis=1)  13.5 us
    all_to_all x1, starting transfers between devices, copy_for_each(): return lax.all_to_all(copies, axis, split_axis=0, concat_axis=0, tiled=True)  13.2 us
    all_to_all x1, waiting for transfers between devices, copy_for_each(): return lax.all_to_all(copies, axis, split_axis=0, concat_axis=0, tiled=True)  12.1 us
    all_gather x1, local copies, waits for them, and re-layouts, on_device(): feature_block = jnp.concatenate(lax.all_gather(layer_input, 'tp'), axis=1)  11.4 us
    unnamed x12, local copies, waits for them, and re-layouts  8.3 us
    dot_general x1, matrix products, on_device(): jnp.dot(feature_block, value_weight, preferred_element_type=jnp.float32)  5.9 us
  transfers between devices with their start and end apart: 3, of which 3 were waited for; matrix products, arithmetic and copies ran while one was open for 5% of the time, Pallas kernels for 0%

profile of v1, /device:TPU:1, one launch (start us, length us, event | category | flops | bytes accessed | tf_op | source)
XLA Modules:
  0.0 200.1 jit_solution(17558376233590204284)
XLA Ops:
  7.2 0.0 copy-start
  7.2 0.0 all-gather.3.cloned.1.call-start
  7.2 0.7 all-gather.3.cloned.1.call-update
  7.9 4.1 %copy.27 = bf16[256,4096]{1,0:T(8,128)(2,1)} copy(bf16[256,4096]{0,1:T(8,128)(2,1)} %bitcast.49) | data formatting | bytes 4194304 | tf_op jit(solution)/shard_map/dot_general | solution.py:53
  12.1 0.7 reshape.164
  12.8 0.7 exp.11
  13.4 0.1 fusion.12
  13.5 0.7 convert_multiply_fusion
  14.2 0.7 multiply_exponential_fusion
  15.0 1.0 multiply_cosine_fusion
  16.0 86.3 %all-gather.3.cloned.1.call-done = bf16[16384,256]{1,0:T(8,128)(2,1)} async-done(((bf16[1024,256]{1,0:T(8,128)(2,1)}), bf16[16384,256]{1,0:T(8,128)(2,1)}) %all-gather.3.cloned.1.call-update) | async-done | bytes 8388624 | tf_op jit(solution)/shard_map/all_gather | solution.py:52
  102.3 7.8 %copy.30 = bf16[128,8,16,256]{3,1,2,0:T(8,128)(2,1)} copy(bf16[128,8,16,256]{3,1,0,2:T(8,128)(2,1)} %bitcast.45) | data formatting | bytes 16777216
  110.0 11.4 %copy.41 = bf16[16,1024,256]{2,0,1:T(8,128)(2,1)} copy(bf16[16,1024,256]{2,1,0:T(8,128)(2,1)} %bitcast.46) | data formatting | bytes 16777216 | tf_op jit(solution)/shard_map/all_gather | solution.py:52
  121.4 13.5 %reshape.159 = bf16[1024,4096,1]{1,0,2:T(8,128)(2,1)} reshape(bf16[1024,16,256]{2,1,0:T(8,128)(2,1)} %bitcast.47) | data formatting | bytes 16777216 | tf_op jit(solution)/shard_map/reshape | solution.py:52
  134.9 0.0 copy-done
  134.9 0.0 copy-start.1
  134.9 0.0 copy-start.2
  134.9 5.9 %convolution_convert_fusion = bf16[1024,256]{0,1:T(8,128)(2,1)S(1)} fusion(bf16[1024,4096]{1,0:T(8,128)(2,1)} %bitcast.48, bf16[4096,256]{1,0:T(8,128)(2,1)S(1)} %copy-done), kind=kOutput, calls=%fused_computation | convolution fusion | flops 2147745792 | bytes 11010048 | tf_op jit(solution)/shard_map/dot_general | solution.py:54
  140.8 0.0 copy-done.1
  140.8 0.4 copy-done.2
  141.2 0.0 copy-start.3
  141.2 0.0 copy-start.4
  141.2 2.4 %fusion.15 = f32[1024,2,128]{0,2,1:T(8,128)S(1)} fusion(bf16[1024,4096,1]{1,0,2:T(8,128)(2,1)S(1)} %copy-done.1, bf16[2,128,4096]{2,1,0:T(8,128)(2,1)S(1)} %bitcast.50), kind=kOutput, calls=%fused_computation.38 | convolution fusion | flops 2147483648 | bytes 11534336 | tf_op jit(solution)/shard_map/dot_general | solution.py:53
  143.6 0.2 multiply_subtract_fusion
  143.8 0.3 fusion.1
  144.1 0.3 fusion.5
  144.4 0.6 broadcast_in_dim.4
  145.1 13.2 %all-to-all-start.1 = ((f32[32,2,2,128]{3,2,1,0:T(2,128)}), f32[32,2,2,128]{3,2,1,0:T(2,128)S(1)}, u32[]{:S(2)}, u32[]{:S(2)}) async-start(f32[32,2,2,128]{3,2,1,0:T(2,128)} %broadcast_in_dim.4), calls=%async_computation.1 | async-start | bytes 131072 | tf_op jit(solution)/shard_map/all_to_all | solution.py:22
  158.2 0.1 broadcast_bitcast_fusion.2
  158.3 0.0 copy-done.3
  158.3 0.1 reduce_sum.44
  158.4 0.8 multiply_convert_fusion.2
  159.2 12.1 %all-to-all-done.1 = f32[32,2,2,128]{3,2,1,0:T(2,128)S(1)} async-done(((f32[32,2,2,128]{3,2,1,0:T(2,128)}), f32[32,2,2,128]{3,2,1,0:T(2,128)S(1)}, u32[]{:S(2)}, u32[]{:S(2)}) %all-to-all-start.1) | async-done | bytes 65568 | tf_op jit(solution)/shard_map/all_to_all | solution.py:22
  171.2 5.1 %all-to-all-start = ((bf16[32,2,2,4,128]{4,3,2,1,0:T(4,128)(2,1)}), bf16[32,2,2,4,128]{4,3,2,1,0:T(4,128)(2,1)S(1)}, u32[]{:S(2)}, u32[]{:S(2)}) async-start(bf16[32,2,2,4,128]{4,3,2,1,0:T(4,128)(2,1)} %multiply_convert_fusion.2), calls=%async_computation | async-start | bytes 262144 | tf_op jit(solution)/shard_map/all_to_all | solution.py:16
  176.4 0.2 broadcast_bitcast_fusion.1
  176.6 0.1 broadcast_bitcast_fusion
  176.6 0.0 copy-done.4
  176.6 0.6 fusion.10
  177.2 15.3 %all-to-all-done = bf16[32,2,2,4,128]{4,3,2,1,0:T(4,128)(2,1)S(1)} async-done(((bf16[32,2,2,4,128]{4,3,2,1,0:T(4,128)(2,1)}), bf16[32,2,2,4,128]{4,3,2,1,0:T(4,128)(2,1)S(1)}, u32[]{:S(2)}, u32[]{:S(2)}) %all-to-all-start) | async-done | bytes 131104 | tf_op jit(solution)/shard_map/all_to_all | solution.py:16
  192.6 0.7 reduce_sum.41
  (8 shorter events, 0.1 us)
Async XLA Ops:
  7.2 127.7 %copy-start = (bf16[4096,256]{1,0:T(8,128)(2,1)S(1)}, bf16[4096,256]{1,0:T(8,128)(2,1)}, u32[]{:S(2)}) copy-start(bf16[4096,256]{1,0:T(8,128)(2,1)} %param.10) | copy-start | bytes 6291460
  7.2 95.1 %all-gather.3.cloned.1.call-start = ((), (), s32[]{:S(2)}) async-start(), calls=%async_computation.2 | async-start | bytes 8912896 | tf_op jit(solution)/shard_map/all_gather | solution.py:52
  134.9 5.9 %copy-start.1 = (bf16[1024,4096,1]{1,0,2:T(8,128)(2,1)S(1)}, bf16[1024,4096,1]{1,0,2:T(8,128)(2,1)}, u32[]{:S(2)}) copy-start(bf16[1024,4096,1]{1,0,2:T(8,128)(2,1)} %reshape.159) | copy-start | bytes 25165828
  134.9 6.4 %copy-start.2 = (bf16[256,4096]{1,0:T(8,128)(2,1)S(1)}, bf16[256,4096]{1,0:T(8,128)(2,1)}, u32[]{:S(2)}) copy-start(bf16[256,4096]{1,0:T(8,128)(2,1)} %copy.27) | copy-start | bytes 6291460
  141.2 17.1 %copy-start.3 = (bf16[2,256]{1,0:T(2,128)(2,1)S(1)}, bf16[2,256]{1,0:T(2,128)(2,1)}, u32[]{:S(2)}) copy-start(bf16[2,256]{1,0:T(2,128)(2,1)} %param.14) | copy-start | bytes 3076
  141.2 35.4 %copy-start.4 = (f32[256]{0:T(256)S(1)}, f32[256]{0:T(256)}, u32[]{:S(2)}) copy-start(f32[256]{0:T(256)} %param.15) | copy-start | bytes 3076
  145.1 26.2 %all-to-all-start.1 = ((f32[32,2,2,128]{3,2,1,0:T(2,128)}), f32[32,2,2,128]{3,2,1,0:T(2,128)S(1)}, u32[]{:S(2)}, u32[]{:S(2)}) async-start(f32[32,2,2,128]{3,2,1,0:T(2,128)} %broadcast_in_dim.4), calls=%async_computation.1 | async-start | bytes 131072 | tf_op jit(solution)/shard_map/all_to_all | solution.py:22
  171.2 21.3 %all-to-all-start = ((bf16[32,2,2,4,128]{4,3,2,1,0:T(4,128)(2,1)}), bf16[32,2,2,4,128]{4,3,2,1,0:T(4,128)(2,1)S(1)}, u32[]{:S(2)}, u32[]{:S(2)}) async-start(bf16[32,2,2,4,128]{4,3,2,1,0:T(4,128)(2,1)} %multiply_convert_fusion.2), calls=%async_computation | async-start | bytes 262144 | tf_op jit(solution)/shard_map/all_to_all | solution.py:16
Sparse Core Ops, SparseCore 0:
  11.0 91.2 all-gather.2
